TPU v7x, 32 devices: a whole 2x2x4 slice. The times are simulated.
32 devices in a mesh: ep: 8 (over z, core), tp: 4 (over y, x).
Axes of the slice: x: 2, y: 2, z: 4, core: 2. Of those that a mesh axis runs over, the one named last changes fastest.
Arguments:
- query_in: bfloat16 [1024, 8192], P('tp', 'ep'), may hold values from -6 to 6
- key_in: bfloat16 [1024, 8192], P('tp', 'ep'), may hold values from -10 to 10
- value_in: bfloat16 [1024, 8192], P('tp', 'ep'), may hold values from -6 to 6
- erase_pre: bfloat16 [1024, 8192], P('tp', 'ep'), may hold values from -8 to 5
- decay_pre: bfloat16 [1024, 8192], P('tp', 'ep'), may hold values from -30 to 4.5
- mix_gain: float32 [1024], P('tp'), may hold values from 0.1 to 1.9
- expert_in: bfloat16 [2048, 2048], P('ep'), may hold values from -6 to 6
- expert_gain: float32 [2048], replicated, may hold values from 0.1 to 1.9
- routes: int32 [2048, 2], P('ep'), may hold values from 0 to 7, all different within a row; in each aligned block of 256 rows (0 to 255, 256 to 511, ...) at most 96 rows name the same one
- route_weight: float32 [2048, 2], P('ep'), may hold values from 0.1 to 1
- gate_weight: bfloat16 [8, 2048, 3584], P('ep', None, 'tp'), may hold values from -0.125 to 0.125
- up_weight: bfloat16 [8, 2048, 3584], P('ep', None, 'tp'), may hold values from -0.125 to 0.125
- down_weight: bfloat16 [8, 3584, 2048], P('ep', 'tp'), may hold values from -0.09375 to 0.09375
Outputs:
- mixer_out: bfloat16 [1024, 8192], P('tp', 'ep')
- expert_out: bfloat16 [2048, 2048], P('ep', 'tp')
Inputs may be any that keep to these rules, and one draw needn't show every extreme that they name: `routes`: A row's 2 experts differ. Within the 256 rows of one index of ep, every expert is named at most 96 times; in some of these aligned blocks one expert is named exactly 96 times.
All inputs are finite; a program needn't handle non-finite values.
Results may differ from a plain program's by a relative error of at most 0.015.
Values may be sent and summed in bfloat16 or wider, within the bound.
A program may use at most 128 MiB of HBM per device.

v0:
```python
import math

import jax
import jax.numpy as jnp
from jax import lax
from jax.experimental import pallas as pl
from jax.experimental.pallas import tpu as pltpu
from jax.sharding import PartitionSpec as P

HEAD_DIM = 64


highest = lax.Precision.HIGHEST
SPAN = 128


def dot(left, right, dims=((1,), (0,)), precision=None):
    return lax.dot_general(
        left, right, (dims, ((), ())), precision=precision, preferred_element_type=jnp.float32
    )


def low(array):
    return array.astype(jnp.bfloat16)


TN = ((0,), (0,))
NT = ((1,), (1,))


def local_kernel(q_ref, k_ref, v_ref, e_ref, d_ref, read_ref, out_ref, step_ref, map_ref):
    channels, span = q_ref.shape
    heads = channels // HEAD_DIM
    row = lax.broadcasted_iota(jnp.int32, (span, span), 0)
    col = lax.broadcasted_iota(jnp.int32, (span, span), 1)
    crossed = row ^ col

    query_f = q_ref[...].astype(jnp.float32)
    key_f = k_ref[...].astype(jnp.float32)
    value = v_ref[...]
    log_keep = -math.exp(-0.5) / (1.0 + jnp.exp(-d_ref[...].astype(jnp.float32)))
    squares = (key_f * key_f).reshape(heads, HEAD_DIM, span)
    norm = lax.rsqrt(jnp.sum(squares, axis=1, keepdims=True) + 1e-05)
    unit = (key_f.reshape(heads, HEAD_DIM, span) * norm).reshape(channels, span)
    eraser = unit / (1.0 + jnp.exp(-e_ref[...].astype(jnp.float32)))

    upper = jnp.where(row <= col, 1.0, 0.0)
    cumulative = dot(log_keep, upper, precision=highest)
    prior = cumulative - log_keep
    total = cumulative[:, span - 1 :]
    middle = cumulative[:, span // 2 - 1 : span // 2]
    prior_up = jnp.exp(prior - middle)
    cum_down = jnp.exp(middle - cumulative)
    cum_up = jnp.exp(cumulative - middle)
    prior_down = jnp.exp(middle - prior)
    to_middle = jnp.exp(middle)
    from_middle = jnp.exp(total - middle)
    decay = jnp.exp(total)

    sides = (
        (unit * prior_up, query_f * cum_up, key_f * cum_down, eraser * cum_down,
         to_middle, from_middle, row < col, row <= col),
        (unit * cum_down, query_f * prior_down, key_f * prior_up, eraser * prior_up,
         from_middle, to_middle, row > col, row >= col),
    )
    units = []
    for side, (u, q, k, e, scale_in, scale_out, strict, inclusive) in enumerate(sides):
        u0, q0 = u * scale_in, q * scale_in
        for h in range(heads):
            at = slice(h * HEAD_DIM, (h + 1) * HEAD_DIM)
            uq = jnp.concatenate([low(u[at]), low(q[at])], axis=1)
            kb, eb = low(k[at]), low(e[at])
            mk = dot(kb, uq, TN)
            me = dot(eb, uq, TN)
            erase_mix = jnp.where(strict, me[:, :span], 0.0)
            units.append(
                dict(
                    side=side, h=h, at=at, kb=kb, eb=eb, u0=u0[at], q0=q0[at],
                    key_mix=low(jnp.where(strict, mk[:, :span], 0.0)),
                    key_read=low(jnp.where(inclusive, mk[:, span:], 0.0)),
                    erase_read=low(jnp.where(inclusive, me[:, span:], 0.0)),
                    erase_mix=erase_mix,
                    scale_out=scale_out[at], decay=decay[at],
                )
            )
    eye = jnp.where(row == col, 1.0, 0.0)
    solved = [eye - jnp.where(crossed == 1, m["erase_mix"], 0.0) for m in units]
    level = 1
    while (1 << level) < span:
        mask = (crossed >> level) == 1
        held = [low(x) for x in solved]
        half = [
            low(dot(x, low(jnp.where(mask, m["erase_mix"], 0.0)))) for x, m in zip(held, units)
        ]
        solved = [s - dot(y, x) for s, y, x in zip(solved, half, held)]
        level += 1

    outs = [None] * heads
    eye_k = jnp.where(
        lax.broadcasted_iota(jnp.int32, (HEAD_DIM, HEAD_DIM), 0)
        == lax.broadcasted_iota(jnp.int32, (HEAD_DIM, HEAD_DIM), 1),
        1.0,
        0.0,
    )
    for m, x in zip(units, solved):
        v = value[m["at"]]
        vm = dot(v, jnp.concatenate([m["key_mix"], m["key_read"]], axis=1))
        stacked = jnp.concatenate([low(vm[:, :span]), low(m["u0"])], axis=0)
        removed = low(dot(stacked, low(x)))
        taken = dot(removed, m["erase_read"])
        local = vm[:, span:] - taken[:HEAD_DIM]
        h, side = m["h"], m["side"]
        outs[h] = local if outs[h] is None else outs[h] + local
        read_ref[side, m["at"], :] = low(m["q0"] - taken[HEAD_DIM:])
        gone = dot(m["eb"], removed, NT)
        added = dot(m["kb"], v, NT)
        state = (added - gone[:, :HEAD_DIM]) * m["scale_out"]
        moved = eye_k * m["decay"] - gone[:, HEAD_DIM:] * m["scale_out"]
        step_ref[0, side, h] = jnp.concatenate([state, moved], axis=1)
    for h in range(heads):
        out_ref[h * HEAD_DIM : (h + 1) * HEAD_DIM, :] = outs[h]

    first = pl.program_id(0) == 0

    @pl.when(first)
    def _():
        map_ref[...] = step_ref[0]

    @pl.when(jnp.logical_not(first))
    def _():
        for h in range(heads):
            step = step_ref[0, 0, h]
            new = dot(step[:, HEAD_DIM:], map_ref[0, h], precision=highest)
            map_ref[0, h] = new + jnp.concatenate(
                [step[:, :HEAD_DIM], jnp.zeros_like(eye_k)], axis=1
            )
            before = map_ref[1, h]
            new = dot(before[:, HEAD_DIM:], step_ref[0, 1, h], precision=highest)
            map_ref[1, h] = new + jnp.concatenate(
                [before[:, :HEAD_DIM], jnp.zeros_like(eye_k)], axis=1
            )


def finish_kernel(maps_ref, step_ref, read_ref, local_ref, gain_ref, out_ref, enter_ref, states_ref):
    count = maps_ref.shape[0]
    heads = maps_ref.shape[2]
    blocks = step_ref.shape[0]
    mine = lax.axis_index("ep")
    enter_ref[...] = jnp.zeros_like(enter_ref)

    def gather(j, carry):
        for side, at in ((0, j), (1, count - 1 - j)):
            reached = at < mine if side == 0 else at > mine

            @pl.when(reached)
            def _():
                for h in range(heads):
                    part = maps_ref[at, side, h]
                    state = enter_ref[side, h]
                    high = low(state)
                    rest = low(state - high.astype(jnp.float32))
                    both = jnp.concatenate([high, rest], axis=1)
                    new = dot(part[:, HEAD_DIM:], both)
                    enter_ref[side, h] = (
                        new[:, :HEAD_DIM] + new[:, HEAD_DIM:] + part[:, :HEAD_DIM].astype(jnp.float32)
                    )

        return carry

    lax.fori_loop(0, count, gather, 0)

    def chain(j, carry):
        for side, at in ((0, j), (1, blocks - 1 - j)):
            for h in range(heads):
                step = step_ref[at, side, h]
                state = enter_ref[side, h]
                states_ref[at, h, side * HEAD_DIM : (side + 1) * HEAD_DIM, :] = low(state)
                enter_ref[side, h] = step[:, :HEAD_DIM] + dot(
                    step[:, HEAD_DIM:], state, precision=highest
                )
        return carry

    lax.fori_loop(0, blocks, chain, 0)

    def write(j, carry):
        tokens = pl.ds(pl.multiple_of(j * SPAN, SPAN), SPAN)
        for h in range(heads):
            at = slice(h * HEAD_DIM, (h + 1) * HEAD_DIM)
            reads = jnp.concatenate([read_ref[0, at, tokens], read_ref[1, at, tokens]], axis=0)
            summed = local_ref[at, tokens] + dot(states_ref[j, h], reads, TN)
            center = jnp.mean(summed, axis=0, keepdims=True)
            moved = summed - center
            spread = jnp.mean(moved * moved, axis=0, keepdims=True)
            scaled = moved * lax.rsqrt(spread + HEAD_DIM * 1e-05) * gain_ref[at, :]
            out_ref[at, tokens] = low(scaled)
        return carry

    lax.fori_loop(0, blocks, write, 0)


def mixer_local(query_in, key_in, value_in, erase_pre, decay_pre):
    channels, seq_len = query_in.shape
    heads = channels // HEAD_DIM
    blocks = seq_len // SPAN
    taken = pl.BlockSpec((channels, SPAN), lambda c: (0, c))
    f32 = jnp.float32
    reads, local, steps, maps = pl.pallas_call(
        local_kernel,
        grid=(blocks,),
        in_specs=[taken] * 5,
        out_specs=[
            pl.BlockSpec((2, channels, SPAN), lambda c: (0, 0, c)),
            taken,
            pl.BlockSpec((1, 2, heads, HEAD_DIM, 2 * HEAD_DIM), lambda c: (c, 0, 0, 0, 0)),
            pl.BlockSpec((2, heads, HEAD_DIM, 2 * HEAD_DIM), lambda c: (0, 0, 0, 0)),
        ],
        out_shape=[
            jax.ShapeDtypeStruct((2, channels, seq_len), jnp.bfloat16),
            jax.ShapeDtypeStruct((channels, seq_len), f32),
            jax.ShapeDtypeStruct((blocks, 2, heads, HEAD_DIM, 2 * HEAD_DIM), f32),
            jax.ShapeDtypeStruct((2, heads, HEAD_DIM, 2 * HEAD_DIM), f32),
        ],
        compiler_params=pltpu.CompilerParams(dimension_semantics=("arbitrary",)),
        cost_estimate=pl.CostEstimate(
            flops=int(4e10 * heads * blocks / 32), bytes_accessed=1 << 23, transcendentals=1 << 20
        ),
        name="mixer_local",
    )(query_in, key_in, value_in, erase_pre, decay_pre)
    return reads, local, steps, maps


def mixer_finish(gathered, steps, reads, local, mix_gain):
    channels, seq_len = local.shape
    blocks, _, heads = steps.shape[:3]
    f32 = jnp.float32
    return pl.pallas_call(
        finish_kernel,
        out_shape=jax.ShapeDtypeStruct((channels, seq_len), jnp.bfloat16),
        scratch_shapes=[
            pltpu.VMEM((2, heads, HEAD_DIM, HEAD_DIM), f32),
            pltpu.VMEM((blocks, heads, 2 * HEAD_DIM, HEAD_DIM), jnp.bfloat16),
        ],
        cost_estimate=pl.CostEstimate(
            flops=int(1e10 * heads * blocks / 32), bytes_accessed=1 << 23, transcendentals=1 << 14
        ),
        name="mixer_finish",
    )(gathered, steps, reads, local, mix_gain.reshape(channels, 1))


def slot_targets(routes, experts_n, capacity):
    onehot = (routes[:, :, None] == jnp.arange(experts_n, dtype=jnp.int32)[None, None, :]).astype(
        jnp.int32
    )
    flat = onehot.reshape(-1, experts_n)
    before = jnp.cumsum(flat, axis=0) - flat
    slot_index = jnp.sum(before * flat, axis=-1).reshape(routes.shape)
    return routes * capacity + slot_index


def dispatch_matrix(targets, slot_total):
    matches = targets[None, :, :] == jnp.arange(slot_total, dtype=jnp.int32)[:, None, None]
    return jnp.sum(matches.astype(jnp.float32), axis=-1).astype(jnp.bfloat16)


def expert_half(
    hold, expert_in, expert_gain, routes, route_weight, gate_weight, up_weight, down_weight
):
    experts_n = lax.axis_size("ep")
    row_count = expert_in.shape[0]
    capacity = 3 * routes.shape[1] * row_count // (2 * experts_n)
    slot_total = experts_n * capacity
    input_f = expert_in.astype(jnp.float32)
    normed = (
        input_f
        * lax.rsqrt(jnp.mean(input_f * input_f, axis=-1, keepdims=True) + 1e-06)
        * expert_gain
    ).astype(jnp.bfloat16)
    targets = slot_targets(routes, experts_n, capacity)
    col_count = normed.shape[1] // lax.axis_size("tp")
    mine = lax.dynamic_slice_in_dim(normed, lax.axis_index("tp") * col_count, col_count, 1)
    buffer = jnp.dot(
        dispatch_matrix(targets, slot_total), mine, preferred_element_type=jnp.float32
    ).astype(jnp.bfloat16)
    gate_local = gate_weight[0]
    up_local = up_weight[0]
    down_local = down_weight[0]
    share = lax.all_to_all(
        buffer.reshape(experts_n, capacity, col_count),
        "ep",
        split_axis=0,
        concat_axis=0,
        tiled=True,
    ).reshape(slot_total, col_count)
    arrived = lax.all_gather(share, "tp", axis=1, tiled=True)
    arrived, gathered = hold(arrived)
    gate_sum = jnp.dot(arrived, gate_local, preferred_element_type=jnp.float32)
    up_sum = jnp.dot(arrived, up_local, preferred_element_type=jnp.float32)
    hidden = (jax.nn.silu(gate_sum) * up_sum).astype(jnp.bfloat16)
    partial_sum = lax.dot_general(
        down_local, hidden, (((0,), (1,)), ((), ())), preferred_element_type=jnp.float32
    ).astype(jnp.bfloat16)
    partial_sum, gathered = lax.optimization_barrier((partial_sum, gathered))
    summed = lax.psum_scatter(
        partial_sum,
        "tp",
        scatter_dimension=0,
        tiled=True,
    )
    returned = lax.all_to_all(
        summed.reshape(col_count, experts_n, capacity),
        "ep",
        split_axis=1,
        concat_axis=1,
        tiled=True,
    ).reshape(col_count, slot_total)
    matches = targets[:, :, None] == jnp.arange(slot_total, dtype=jnp.int32)[None, None, :]
    combine = jnp.sum(matches.astype(jnp.float32) * route_weight[:, :, None], axis=1)
    result = jnp.einsum(
        "tx,cx->tc", combine, returned.astype(jnp.float32), precision=highest
    ).astype(jnp.bfloat16)
    return result, gathered


def on_device(
    query_in,
    key_in,
    value_in,
    erase_pre,
    decay_pre,
    mix_gain,
    expert_in,
    expert_gain,
    routes,
    route_weight,
    gate_weight,
    up_weight,
    down_weight,
):
    reads, local, steps, maps = mixer_local(query_in, key_in, value_in, erase_pre, decay_pre)

    def hold(arrived):
        held, sent = lax.optimization_barrier((arrived, maps.astype(jnp.bfloat16)))
        return held, lax.all_gather(sent, "ep")

    expert_out, gathered = expert_half(
        hold, expert_in, expert_gain, routes, route_weight, gate_weight, up_weight, down_weight
    )
    mixer_out = mixer_finish(gathered, steps, reads, local, mix_gain)
    return (mixer_out, expert_out)


def solution(mesh):
    placed = (
        P("tp", "ep"),
        P("tp", "ep"),
        P("tp", "ep"),
        P("tp", "ep"),
        P("tp", "ep"),
        P("tp"),
        P("ep", None),
        P(),
        P("ep", None),
        P("ep", None),
        P("ep", None, "tp"),
        P("ep", None, "tp"),
        P("ep", "tp", None),
    )
    return jax.shard_map(
        on_device,
        mesh=mesh,
        in_specs=placed,
        out_specs=(P("tp", "ep"), P("ep", "tp")),
        check_vma=False,
    )
```

profile of v0, /device:TPU:0, one launch (start us, length us, event | category | flops | bytes accessed | tf_op | source)
XLA Modules:
  0.0 188.2 jit_solution(14446818803116518032)
XLA Ops:
  7.2 0.0 all-gather.4.cloned.1.call-start
  7.2 0.9 copy.37
  8.1 0.1 eq.56
  8.3 0.1 eq.52
  8.4 1.5 convert_element_type.44
  9.9 0.3 multiply_reduce_fusion
  10.2 1.1 reduce-window.6
  11.3 0.2 slice_reduce_fusion
  11.6 0.1 fusion.23
  11.7 0.1 reshape.53
  11.8 0.1 copy.39
  11.9 0.3 convert_reduce_fusion
  12.3 0.8 dynamic-slice
  13.1 0.4 convolution_convert_fusion
  13.5 27.2 %all_to_all.10 = bf16[8,96,512]{2,1,0:T(8,128)(2,1)} all-to-all(bf16[8,96,512]{2,1,0:T(8,128)(2,1)S(1)} %bitcast.40), channel_id=1, replica_groups=mesh['ep'=8,'tp'=4] {'ep'}, dimensions={0} | all-to-all | bytes 1572864 | tf_op jit(solution)/shard_map/all_to_all | solution.py:287
  40.7 0.0 all-gather.4.cloned.1.call-update
  40.7 0.0 all-gather.6.cloned.1.call-start
  40.8 42.5 %mixer_local.1 = (bf16[2,256,1024]{2,1,0:T(8,128)(2,1)}, f32[256,1024]{1,0:T(8,128)}, f32[8,2,4,64,128]{4,3,2,1,0:T(8,128)}, f32[2,4,64,128]{3,2,1,0:T(8,128)}) custom-call(bf16[256,1024]{1,0:T(8,128)(2,1)} %q_ref.1, bf16[256,1024]{1,0:T(8,128)(2,1)} %k_ref.1, bf16[256,1024]{1,0:T(8,128)(2,1)} %v_ref.1, bf16[256,1024]{1,0:T(8,128)(2,1)} %e_ref.1, ...), custom_call_target="tpu_custom_call" | custom-call | flops 40000000000 | bytes 8388608 | tf_op jit(solution)/shard_map/mixer_local/pallas_call | solution.py:207
  83.3 1.6 convert_element_type.47
  84.9 0.0 all-gather.6.cloned.1.call-update
  84.9 0.2 reduce-scatter.2.cloned.1.call-start
  85.2 8.1 %fusion.2 = f32[768,896]{1,0:T(8,128)} fusion(bf16[768,2048]{1,0:T(8,128)(2,1)} %all-gather.4.cloned.1.call-done, bf16[1,2048,896]{2,1,0:T(8,128)(2,1)} %param.24), kind=kOutput, calls=%fused_computation.2 | convolution fusion | flops 2818572288 | bytes 9568256 | tf_op jit(solution)/shard_map/dot_general | solution.py:297
  93.3 12.5 %fusion.9 = bf16[2048,768]{0,1:T(8,128)(2,1)} fusion(bf16[1,896,2048]{2,1,0:T(8,128)(2,1)} %param.25, f32[768,896]{1,0:T(8,128)} %fusion.2, bf16[768,2048]{1,0:T(8,128)(2,1)S(1)} %copy-done.4, bf16[1,2048,896]{2,1,0:T(8,128)(2,1)} %param.23), kind=kOutput, calls=%fused_computation.7 | convolution fusion | flops 5642846208 | bytes 16384000 | tf_op jit(solution)/shard_map/dot_general | solution.py:299
  105.7 2.4 %all-gather.6.cloned.1.call-done = bf16[16,4,64,128]{3,2,1,0:T(8,128)(2,1)} async-done(((bf16[2,4,64,128]{3,2,1,0:T(8,128)(2,1)}), bf16[16,4,64,128]{3,2,1,0:T(8,128)(2,1)}) %all-gather.6.cloned.1.call-update) | async-done | bytes 1048592 | tf_op jit(solution)/shard_map/all_gather | solution.py:343
  108.1 0.0 reduce-scatter.2.cloned.1.call-update
  108.1 46.5 %reduce-scatter.2.cloned.1.call-done = bf16[512,768]{0,1:T(8,128)(2,1)} async-done(((bf16[2048,768]{0,1:T(8,128)(2,1)}), bf16[512,768]{0,1:T(8,128)(2,1)}) %reduce-scatter.2.cloned.1.call-update) | async-done | bytes 786448 | tf_op jit(solution)/shard_map/reduce_scatter | solution.py:303
  154.6 4.6 %all-to-all-start.1 = ((bf16[512,8,96]{0,2,1:T(8,128)(2,1)}), bf16[512,8,96]{0,2,1:T(8,128)(2,1)S(1)}, u32[]{:S(2)}, u32[]{:S(2)}) async-start(bf16[512,8,96]{0,2,1:T(8,128)(2,1)} %bitcast.41), calls=%async_computation.2 | async-start | bytes 1572864 | tf_op jit(solution)/shard_map/all_to_all | solution.py:309
  159.2 0.8 copy.40.gain_ref
  160.0 0.2 select_reduce_fusion
  160.2 11.0 %mixer_finish.1 = bf16[256,1024]{1,0:T(8,128)(2,1)} custom-call(bf16[8,2,4,64,128]{4,3,2,1,0:T(8,128)(2,1)} %bitcast.43, f32[8,2,4,64,128]{4,3,2,1,0:T(8,128)} %get-tuple-element.14.step_ref, bf16[2,256,1024]{2,1,0:T(8,128)(2,1)} %get-tuple-element.15.read_ref, f32[256,1024]{1,0:T(8,128)} %get-tuple-element.16.local_ref, f32[256,1]{1,0:T(8,128)} %copy.40.gain_ref), custom_call_target="tpu_custom_call" | custom-call | flops 10000000000 | bytes 8388608 | tf_op jit(solution)/shard_map/mixer_finish/pallas_call | solution.py:236
  171.3 8.9 %all-to-all-done.1 = bf16[512,8,96]{0,2,1:T(8,128)(2,1)S(1)} async-done(((bf16[512,8,96]{0,2,1:T(8,128)(2,1)}), bf16[512,8,96]{0,2,1:T(8,128)(2,1)S(1)}, u32[]{:S(2)}, u32[]{:S(2)}) %all-to-all-start.1) | async-done | bytes 786464 | tf_op jit(solution)/shard_map/all_to_all | solution.py:309
  180.2 1.5 convolution_convert_fusion.1
  (16 shorter events, 0.1 us)
Async XLA Ops:
  7.2 4.8 %copy-start.1 = (s32[256,2]{0,1:T(2,128)S(1)}, s32[256,2]{0,1:T(2,128)}, u32[]{:S(2)}) copy-start(s32[256,2]{0,1:T(2,128)} %param.21) | copy-start | bytes 6148
  7.2 2.7 %copy-start = (bf16[256,2048]{1,0:T(8,128)(2,1)S(1)}, bf16[256,2048]{1,0:T(8,128)(2,1)}, u32[]{:S(2)}) copy-start(bf16[256,2048]{1,0:T(8,128)(2,1)} %param.19) | copy-start | bytes 3145732
  7.2 77.7 %all-gather.4.cloned.1.call-start = ((), (), s32[]{:S(2)}) async-start(), calls=%async_computation.3 | async-start | bytes 3932160 | tf_op jit(solution)/shard_map/all_gather | solution.py:294
  40.7 67.3 %all-gather.6.cloned.1.call-start = ((), (), s32[]{:S(2)}) async-start(), calls=%async_computation.5 | async-start | bytes 1179648 | tf_op jit(solution)/shard_map/all_gather | solution.py:343
  84.9 8.3 %copy-start.4 = (bf16[768,2048]{1,0:T(8,128)(2,1)S(1)}, bf16[768,2048]{1,0:T(8,128)(2,1)}, u32[]{:S(2)}) copy-start(bf16[768,2048]{1,0:T(8,128)(2,1)} %all-gather.4.cloned.1.call-done) | copy-start | bytes 9437188
  84.9 69.7 %reduce-scatter.2.cloned.1.call-start = ((), (), s32[]{:S(2)}) async-start(), calls=%async_computation.4 | async-start | bytes 3932160 | tf_op jit(solution)/shard_map/reduce_scatter | solution.py:303
  105.7 53.5 %copy-start.3 = (f32[256]{0:T(256)S(1)}, f32[256]{0:T(256)}, u32[]{:S(2)}) copy-start(f32[256]{0:T(256)} %param.18) | copy-start | bytes 3076
  105.7 54.3 %copy-start.2 = (f32[256,2]{0,1:T(2,128)S(1)}, f32[256,2]{0,1:T(2,128)}, u32[]{:S(2)}) copy-start(f32[256,2]{0,1:T(2,128)} %param.22) | copy-start | bytes 6148
  154.6 25.5 %all-to-all-start.1 = ((bf16[512,8,96]{0,2,1:T(8,128)(2,1)}), bf16[512,8,96]{0,2,1:T(8,128)(2,1)S(1)}, u32[]{:S(2)}, u32[]{:S(2)}) async-start(bf16[512,8,96]{0,2,1:T(8,128)(2,1)} %bitcast.41), calls=%async_computation.2 | async-start | bytes 1572864 | tf_op jit(solution)/shard_map/all_to_all | solution.py:309
Sparse Core Ops, SparseCore 0:
  40.8 42.7 all-gather.3
  85.8 22.2 all-gather.5
  111.1 43.5 reduce-scatter.1
where the time goes:
time: 189 us; the launch traced here: 188 us
  waiting for transfers between devices  57.8 us (31%)
  Pallas kernels  53.5 us (28%)
  blocking collectives  27.2 us (14%)
  matrix products  22.5 us (12%)
  between operations  13.9 us (7%)
  other arithmetic  5.21 us (3%)
  starting transfers between devices  4.89 us (3%)
  local copies, waits for them, and re-layouts  3.2 us (2%)
    reduce_scatter x1, waiting for transfers between devices, expert_half(): lax.psum_scatter(partial_sum, 'tp', scatter_dimension=0, tiled=True)  46.5 us
    pallas_call x1, Pallas kernels, mixer_local(): pl.pallas_call(local_kernel, grid=(blocks,), in_specs=[taken] * 5, out_sp...  42.5 us
    all_to_all x1, blocking collectives, expert_half(): lax.all_to_all(buffer.reshape(experts_n, capacity, col_count), 'ep', spli...  27.2 us
    dot_general x1, matrix products, expert_half(): lax.dot_general(down_local, hidden, (((0,), (1,)), ((), ())), preferred_e...  12.5 us
    pallas_call x1, Pallas kernels, mixer_finish(): pl.pallas_call(finish_kernel, out_shape=jax.ShapeDtypeStruct((channels, s...  11 us
    all_to_all x1, waiting for transfers between devices, expert_half(): lax.all_to_all(summed.reshape(col_count, experts_n, capacity), 'ep', spli...  8.89 us
    dot_general x1, matrix products, expert_half(): up_sum = jnp.dot(arrived, up_local, preferred_element_type=jnp.float32)  8.11 us
    all_to_all x1, starting transfers between devices, expert_half(): lax.all_to_all(summed.reshape(col_count, experts_n, capacity), 'ep', spli...  4.59 us
  transfers between devices with their start and end apart: 4, of which 3 were waited for; matrix products, arithmetic and copies ran while one was open for 12% of the time, Pallas kernels for 28%

commit v1 on v0

--- a/solution.py
+++ b/solution.py
@@ -1,3 +1,4 @@
+import functools
 import math
 
 import jax
@@ -12,6 +13,8 @@
 
 highest = lax.Precision.HIGHEST
 SPAN = 128
+GROUPS = 4
+MESH = pl.DeviceIdType.MESH
 
 
 def dot(left, right, dims=((1,), (0,)), precision=None):
@@ -28,21 +31,46 @@
 NT = ((1,), (1,))
 
 
-def local_kernel(q_ref, k_ref, v_ref, e_ref, d_ref, read_ref, out_ref, step_ref, map_ref):
-    channels, span = q_ref.shape
+def flipped(index, bits):
+    bit = 1
+    out = index
+    while bit <= bits:
+        if bits & bit:
+            out = out + bit - 2 * bit * lax.rem(lax.div(index, bit), 2)
+        bit *= 2
+    return out
+
+
+def greet(ep_count, tp_count, mine, column):
+    barrier = pltpu.get_barrier_semaphore()
+    for s in range(1, ep_count):
+        pl.semaphore_signal(
+            barrier, inc=1, device_id={"ep": flipped(mine, s)}, device_id_type=MESH
+        )
+    for p in range(1, tp_count):
+        pl.semaphore_signal(
+            barrier, inc=1, device_id={"tp": flipped(column, p)}, device_id_type=MESH
+        )
+    pl.semaphore_wait(barrier, ep_count + tp_count - 2)
+
+
+def local_block(c, q_ref, k_ref, v_ref, e_ref, d_ref, read_ref, out_ref, step_ref, map_ref):
+    channels = q_ref.shape[0]
+    span = SPAN
     heads = channels // HEAD_DIM
+    tokens = pl.ds(pl.multiple_of(c * span, span), span)
     row = lax.broadcasted_iota(jnp.int32, (span, span), 0)
     col = lax.broadcasted_iota(jnp.int32, (span, span), 1)
     crossed = row ^ col
 
-    query_f = q_ref[...].astype(jnp.float32)
-    key_f = k_ref[...].astype(jnp.float32)
-    value = v_ref[...]
-    log_keep = -math.exp(-0.5) / (1.0 + jnp.exp(-d_ref[...].astype(jnp.float32)))
+    query_f = q_ref[:, tokens].astype(jnp.float32)
+    key_f = k_ref[:, tokens].astype(jnp.float32)
+    value = v_ref[:, tokens]
+    log_keep = -math.exp(-0.5) / (1.0 + jnp.exp(-d_ref[:, tokens].astype(jnp.float32)))
     squares = (key_f * key_f).reshape(heads, HEAD_DIM, span)
     norm = lax.rsqrt(jnp.sum(squares, axis=1, keepdims=True) + 1e-05)
     unit = (key_f.reshape(heads, HEAD_DIM, span) * norm).reshape(channels, span)
-    eraser = unit / (1.0 + jnp.exp(-e_ref[...].astype(jnp.float32)))
+    eraser = unit / (1.0 + jnp.exp(-e_ref[:, tokens].astype(jnp.float32)))
 
     upper = jnp.where(row <= col, 1.0, 0.0)
     cumulative = dot(log_keep, upper, precision=highest)
@@ -111,51 +139,199 @@
         local = vm[:, span:] - taken[:HEAD_DIM]
         h, side = m["h"], m["side"]
         outs[h] = local if outs[h] is None else outs[h] + local
-        read_ref[side, m["at"], :] = low(m["q0"] - taken[HEAD_DIM:])
+        read_ref[side, m["at"], tokens] = low(m["q0"] - taken[HEAD_DIM:])
         gone = dot(m["eb"], removed, NT)
         added = dot(m["kb"], v, NT)
         state = (added - gone[:, :HEAD_DIM]) * m["scale_out"]
         moved = eye_k * m["decay"] - gone[:, HEAD_DIM:] * m["scale_out"]
-        step_ref[0, side, h] = jnp.concatenate([state, moved], axis=1)
+        step_ref[c, side, h] = jnp.concatenate([state, moved], axis=1)
     for h in range(heads):
-        out_ref[h * HEAD_DIM : (h + 1) * HEAD_DIM, :] = outs[h]
-
-    first = pl.program_id(0) == 0
-
-    @pl.when(first)
-    def _():
-        map_ref[...] = step_ref[0]
-
-    @pl.when(jnp.logical_not(first))
-    def _():
-        for h in range(heads):
-            step = step_ref[0, 0, h]
-            new = dot(step[:, HEAD_DIM:], map_ref[0, h], precision=highest)
-            map_ref[0, h] = new + jnp.concatenate(
-                [step[:, :HEAD_DIM], jnp.zeros_like(eye_k)], axis=1
+        out_ref[h * HEAD_DIM : (h + 1) * HEAD_DIM, tokens] = outs[h]
+
+    none = jnp.zeros_like(eye_k)
+    for h in range(heads):
+        step = step_ref[c, 0, h]
+        new = dot(step[:, HEAD_DIM:], map_ref[0, h], precision=highest)
+        map_ref[0, h] = new + jnp.concatenate([step[:, :HEAD_DIM], none], axis=1)
+        before = map_ref[1, h]
+        new = dot(before[:, HEAD_DIM:], step_ref[c, 1, h], precision=highest)
+        map_ref[1, h] = new + jnp.concatenate([before[:, :HEAD_DIM], none], axis=1)
+
+
+def outbound_kernel(
+    ep_count, tp_count, buffer_ref, q_ref, k_ref, v_ref, e_ref, d_ref,
+    arrived_ref, read_ref, out_ref, step_ref, sent_map_ref,
+    map_ref, own_sem, send_z, recv_z, send_t, recv_t,
+):
+    mine, column = lax.axis_index("ep"), lax.axis_index("tp")
+    blocks = q_ref.shape[1] // SPAN
+    width = buffer_ref.shape[2]
+    groups = min(GROUPS, ep_count)
+    per = ep_count // groups
+    part = pl.ds(pl.multiple_of(column * width, width), width)
+    greet(ep_count, tp_count, mine, column)
+
+    away = {}
+    for s in range(1, ep_count):
+        target = flipped(mine, s)
+        away[s] = pltpu.make_async_remote_copy(
+            src_ref=buffer_ref.at[target],
+            dst_ref=arrived_ref.at[mine, :, part],
+            send_sem=send_z.at[s],
+            recv_sem=recv_z.at[s],
+            device_id={"ep": target},
+            device_id_type=MESH,
+        )
+        away[s].start()
+    own = pltpu.make_async_copy(buffer_ref.at[mine], arrived_ref.at[mine, :, part], own_sem)
+    own.start()
+    own.wait()
+
+    spread = []
+    for k in range(groups):
+        first = flipped(lax.div(mine, per), k) * per
+        block = arrived_ref.at[pl.ds(first, per), :, part]
+        spread.append(
+            [
+                pltpu.make_async_remote_copy(
+                    src_ref=block,
+                    dst_ref=block,
+                    send_sem=send_t.at[k, p],
+                    recv_sem=recv_t.at[k, p],
+                    device_id={"tp": flipped(column, p)},
+                    device_id_type=MESH,
+                )
+                for p in range(1, tp_count)
+            ]
+        )
+
+    def pass_on(k):
+        for s in range(max(1, k * per), (k + 1) * per):
+            away[s].wait_recv()
+        for copy in spread[k]:
+            copy.start()
+
+    pass_on(0)
+    for h in range(map_ref.shape[1]):
+        start = jnp.concatenate(
+            [
+                jnp.zeros((HEAD_DIM, HEAD_DIM), jnp.float32),
+                jnp.where(
+                    lax.broadcasted_iota(jnp.int32, (HEAD_DIM, HEAD_DIM), 0)
+                    == lax.broadcasted_iota(jnp.int32, (HEAD_DIM, HEAD_DIM), 1),
+                    1.0,
+                    0.0,
+                ),
+            ],
+            axis=1,
+        )
+        map_ref[0, h] = start
+        map_ref[1, h] = start
+
+    when = [min(e, blocks - 1) for e in (0, 1, 2, 4)]
+
+    def work(c, carry):
+        for k in range(1, groups):
+
+            @pl.when(c == when[k])
+            def _():
+                pass_on(k)
+
+        local_block(c, q_ref, k_ref, v_ref, e_ref, d_ref, read_ref, out_ref, step_ref, map_ref)
+        return carry
+
+    lax.fori_loop(0, blocks, work, 0)
+    sent_map_ref[...] = low(map_ref[...])
+    for k in range(groups):
+        for copy in spread[k]:
+            copy.wait_recv()
+            copy.wait_send()
+    for s in range(1, ep_count):
+        away[s].wait_send()
+
+
+def inbound_kernel(
+    ep_count, tp_count, part_ref, maps_ref, step_ref, read_ref, local_ref, gain_ref,
+    out_ref, returned_ref,
+    total_ref, peers_ref, gathered_ref, enter_ref, states_ref,
+    send_m, recv_m, send_t, recv_t, send_z, recv_z,
+):
+    mine, column = lax.axis_index("ep"), lax.axis_index("tp")
+    heads = maps_ref.shape[1]
+    blocks = step_ref.shape[0]
+    width = returned_ref.shape[2]
+    groups = min(GROUPS, ep_count)
+    per = ep_count // groups
+    greet(ep_count, tp_count, mine, column)
+
+    order = list(range(groups))[::-1]
+    shares = {}
+    for k in order:
+        rows = pl.ds(flipped(lax.div(mine, per), k) * per, per)
+        for p in range(1, tp_count):
+            target = flipped(column, p)
+            shares[k, p] = pltpu.make_async_remote_copy(
+                src_ref=part_ref.at[rows, :, pl.ds(pl.multiple_of(target * width, width), width)],
+                dst_ref=peers_ref.at[p - 1, rows],
+                send_sem=send_t.at[k, p],
+                recv_sem=recv_t.at[k, p],
+                device_id={"tp": target},
+                device_id_type=MESH,
             )
-            before = map_ref[1, h]
-            new = dot(before[:, HEAD_DIM:], step_ref[0, 1, h], precision=highest)
-            map_ref[1, h] = new + jnp.concatenate(
-                [before[:, :HEAD_DIM], jnp.zeros_like(eye_k)], axis=1
-            )
-
-
-def finish_kernel(maps_ref, step_ref, read_ref, local_ref, gain_ref, out_ref, enter_ref, states_ref):
-    count = maps_ref.shape[0]
-    heads = maps_ref.shape[2]
-    blocks = step_ref.shape[0]
-    mine = lax.axis_index("ep")
+            shares[k, p].start()
+    sides = {}
+    for s in range(1, ep_count):
+        target = lax.rem(mine + s, ep_count)
+        sides[s] = pltpu.make_async_remote_copy(
+            src_ref=maps_ref.at[lax.div(mine + s, ep_count)],
+            dst_ref=gathered_ref.at[mine],
+            send_sem=send_m.at[s],
+            recv_sem=recv_m.at[s],
+            device_id={"ep": target},
+            device_id_type=MESH,
+        )
+        sides[s].start()
+
+    back = {}
+    for s in range(1, ep_count):
+        target = flipped(mine, s)
+        back[s] = pltpu.make_async_remote_copy(
+            src_ref=total_ref.at[target],
+            dst_ref=returned_ref.at[mine],
+            send_sem=send_z.at[s],
+            recv_sem=recv_z.at[s],
+            device_id={"ep": target},
+            device_id_type=MESH,
+        )
+
+    def give_back(k):
+        first = flipped(lax.div(mine, per), k) * per
+        for p in range(1, tp_count):
+            shares[k, p].wait_recv()
+        for r in range(per):
+            own = pl.ds(pl.multiple_of(column * width, width), width)
+            total = part_ref[first + r, :, own].astype(jnp.float32)
+            for p in range(1, tp_count):
+                total = total + peers_ref[p - 1, first + r].astype(jnp.float32)
+            total_ref[first + r] = low(total)
+        for s in range(k * per, (k + 1) * per):
+            if s:
+                back[s].start()
+            else:
+                returned_ref[mine] = total_ref[mine]
+
     enter_ref[...] = jnp.zeros_like(enter_ref)
+    for s in range(1, ep_count):
+        sides[s].wait_recv()
 
     def gather(j, carry):
-        for side, at in ((0, j), (1, count - 1 - j)):
+        for side, at in ((0, j), (1, ep_count - 1 - j)):
             reached = at < mine if side == 0 else at > mine
 
             @pl.when(reached)
             def _():
                 for h in range(heads):
-                    part = maps_ref[at, side, h]
+                    part = gathered_ref[at, h]
                     state = enter_ref[side, h]
                     high = low(state)
                     rest = low(state - high.astype(jnp.float32))
@@ -167,7 +343,7 @@
 
         return carry
 
-    lax.fori_loop(0, count, gather, 0)
+    lax.fori_loop(0, ep_count, gather, 0)
 
     def chain(j, carry):
         for side, at in ((0, j), (1, blocks - 1 - j)):
@@ -182,7 +358,17 @@
 
     lax.fori_loop(0, blocks, chain, 0)
 
+    when = {order[0]: 0}
+    if groups > 1:
+        when[order[1]] = blocks // 2
+
     def write(j, carry):
+        for k, at in when.items():
+
+            @pl.when(j == at)
+            def _():
+                give_back(k)
+
         tokens = pl.ds(pl.multiple_of(j * SPAN, SPAN), SPAN)
         for h in range(heads):
             at = slice(h * HEAD_DIM, (h + 1) * HEAD_DIM)
@@ -196,55 +382,91 @@
         return carry
 
     lax.fori_loop(0, blocks, write, 0)
-
-
-def mixer_local(query_in, key_in, value_in, erase_pre, decay_pre):
+    for k in order:
+        if k not in when:
+            give_back(k)
+    for s in range(1, ep_count):
+        back[s].wait_recv()
+        back[s].wait_send()
+        sides[s].wait_send()
+    for copy in shares.values():
+        copy.wait_send()
+
+
+def outbound(buffer, query_in, key_in, value_in, erase_pre, decay_pre):
     channels, seq_len = query_in.shape
+    ep_count, capacity, width = buffer.shape
+    tp_count = lax.axis_size("tp")
     heads = channels // HEAD_DIM
     blocks = seq_len // SPAN
-    taken = pl.BlockSpec((channels, SPAN), lambda c: (0, c))
+    groups = min(GROUPS, ep_count)
     f32 = jnp.float32
-    reads, local, steps, maps = pl.pallas_call(
-        local_kernel,
-        grid=(blocks,),
-        in_specs=[taken] * 5,
-        out_specs=[
-            pl.BlockSpec((2, channels, SPAN), lambda c: (0, 0, c)),
-            taken,
-            pl.BlockSpec((1, 2, heads, HEAD_DIM, 2 * HEAD_DIM), lambda c: (c, 0, 0, 0, 0)),
-            pl.BlockSpec((2, heads, HEAD_DIM, 2 * HEAD_DIM), lambda c: (0, 0, 0, 0)),
-        ],
+    whole = pl.BlockSpec(memory_space=pltpu.VMEM)
+    dma = pltpu.SemaphoreType.DMA
+    return pl.pallas_call(
+        functools.partial(outbound_kernel, ep_count, tp_count),
+        in_specs=[whole] * 6,
+        out_specs=[whole] * 5,
         out_shape=[
+            jax.ShapeDtypeStruct((ep_count, capacity, width * tp_count), jnp.bfloat16),
             jax.ShapeDtypeStruct((2, channels, seq_len), jnp.bfloat16),
             jax.ShapeDtypeStruct((channels, seq_len), f32),
             jax.ShapeDtypeStruct((blocks, 2, heads, HEAD_DIM, 2 * HEAD_DIM), f32),
-            jax.ShapeDtypeStruct((2, heads, HEAD_DIM, 2 * HEAD_DIM), f32),
+            jax.ShapeDtypeStruct((2, heads, HEAD_DIM, 2 * HEAD_DIM), jnp.bfloat16),
         ],
-        compiler_params=pltpu.CompilerParams(dimension_semantics=("arbitrary",)),
+        scratch_shapes=[
+            pltpu.VMEM((2, heads, HEAD_DIM, 2 * HEAD_DIM), f32),
+            dma,
+            dma((ep_count,)),
+            dma((ep_count,)),
+            dma((groups, tp_count)),
+            dma((groups, tp_count)),
+        ],
+        compiler_params=pltpu.CompilerParams(collective_id=0, has_side_effects=True),
         cost_estimate=pl.CostEstimate(
             flops=int(4e10 * heads * blocks / 32), bytes_accessed=1 << 23, transcendentals=1 << 20
         ),
-        name="mixer_local",
-    )(query_in, key_in, value_in, erase_pre, decay_pre)
-    return reads, local, steps, maps
-
-
-def mixer_finish(gathered, steps, reads, local, mix_gain):
+        name="outbound",
+    )(buffer, query_in, key_in, value_in, erase_pre, decay_pre)
+
+
+def inbound(part, maps, steps, reads, local, mix_gain):
     channels, seq_len = local.shape
+    ep_count, capacity, features = part.shape
+    tp_count = lax.axis_size("tp")
+    width = features // tp_count
     blocks, _, heads = steps.shape[:3]
+    groups = min(GROUPS, ep_count)
     f32 = jnp.float32
+    whole = pl.BlockSpec(memory_space=pltpu.VMEM)
+    dma = pltpu.SemaphoreType.DMA
     return pl.pallas_call(
-        finish_kernel,
-        out_shape=jax.ShapeDtypeStruct((channels, seq_len), jnp.bfloat16),
+        functools.partial(inbound_kernel, ep_count, tp_count),
+        in_specs=[whole] * 6,
+        out_specs=[whole] * 2,
+        out_shape=[
+            jax.ShapeDtypeStruct((channels, seq_len), jnp.bfloat16),
+            jax.ShapeDtypeStruct((ep_count, capacity, width), jnp.bfloat16),
+        ],
         scratch_shapes=[
+            pltpu.VMEM((ep_count, capacity, width), jnp.bfloat16),
+            pltpu.VMEM((tp_count - 1, ep_count, capacity, width), jnp.bfloat16),
+            pltpu.VMEM((ep_count, heads, HEAD_DIM, 2 * HEAD_DIM), jnp.bfloat16),
             pltpu.VMEM((2, heads, HEAD_DIM, HEAD_DIM), f32),
             pltpu.VMEM((blocks, heads, 2 * HEAD_DIM, HEAD_DIM), jnp.bfloat16),
+            dma((ep_count,)),
+            dma((ep_count,)),
+            dma((groups, tp_count)),
+            dma((groups, tp_count)),
+            dma((ep_count,)),
+            dma((ep_count,)),
         ],
+        compiler_params=pltpu.CompilerParams(collective_id=1, has_side_effects=True),
         cost_estimate=pl.CostEstimate(
             flops=int(1e10 * heads * blocks / 32), bytes_accessed=1 << 23, transcendentals=1 << 14
         ),
-        name="mixer_finish",
-    )(gathered, steps, reads, local, mix_gain.reshape(channels, 1))
+        name="inbound",
+    )(part, maps, steps, reads, local, mix_gain.reshape(channels, 1))
 
 
 def slot_targets(routes, experts_n, capacity):
@@ -262,8 +484,20 @@
     return jnp.sum(matches.astype(jnp.float32), axis=-1).astype(jnp.bfloat16)
 
 
-def expert_half(
-    hold, expert_in, expert_gain, routes, route_weight, gate_weight, up_weight, down_weight
+def on_device(
+    query_in,
+    key_in,
+    value_in,
+    erase_pre,
+    decay_pre,
+    mix_gain,
+    expert_in,
+    expert_gain,
+    routes,
+    route_weight,
+    gate_weight,
+    up_weight,
+    down_weight,
 ):
     experts_n = lax.axis_size("ep")
     row_count = expert_in.shape[0]
@@ -281,72 +515,23 @@
     buffer = jnp.dot(
         dispatch_matrix(targets, slot_total), mine, preferred_element_type=jnp.float32
     ).astype(jnp.bfloat16)
-    gate_local = gate_weight[0]
-    up_local = up_weight[0]
-    down_local = down_weight[0]
-    share = lax.all_to_all(
+    arrived, reads, local, steps, maps = outbound(
         buffer.reshape(experts_n, capacity, col_count),
-        "ep",
-        split_axis=0,
-        concat_axis=0,
-        tiled=True,
-    ).reshape(slot_total, col_count)
-    arrived = lax.all_gather(share, "tp", axis=1, tiled=True)
-    arrived, gathered = hold(arrived)
-    gate_sum = jnp.dot(arrived, gate_local, preferred_element_type=jnp.float32)
-    up_sum = jnp.dot(arrived, up_local, preferred_element_type=jnp.float32)
+        query_in, key_in, value_in, erase_pre, decay_pre,
+    )
+    arrived = arrived.reshape(slot_total, -1)
+    gate_sum = jnp.dot(arrived, gate_weight[0], preferred_element_type=jnp.float32)
+    up_sum = jnp.dot(arrived, up_weight[0], preferred_element_type=jnp.float32)
     hidden = (jax.nn.silu(gate_sum) * up_sum).astype(jnp.bfloat16)
-    partial_sum = lax.dot_general(
-        down_local, hidden, (((0,), (1,)), ((), ())), preferred_element_type=jnp.float32
-    ).astype(jnp.bfloat16)
-    partial_sum, gathered = lax.optimization_barrier((partial_sum, gathered))
-    summed = lax.psum_scatter(
-        partial_sum,
-        "tp",
-        scatter_dimension=0,
-        tiled=True,
-    )
-    returned = lax.all_to_all(
-        summed.reshape(col_count, experts_n, capacity),
-        "ep",
-        split_axis=1,
-        concat_axis=1,
-        tiled=True,
-    ).reshape(col_count, slot_total)
+    part = jnp.dot(hidden, down_weight[0], preferred_element_type=jnp.float32).astype(jnp.bfloat16)
+    mixer_out, returned = inbound(
+        part.reshape(experts_n, capacity, -1), maps, steps, reads, local, mix_gain
+    )
+    returned = returned.reshape(slot_total, col_count)
     matches = targets[:, :, None] == jnp.arange(slot_total, dtype=jnp.int32)[None, None, :]
     combine = jnp.sum(matches.astype(jnp.float32) * route_weight[:, :, None], axis=1)
-    result = jnp.einsum(
-        "tx,cx->tc", combine, returned.astype(jnp.float32), precision=highest
-    ).astype(jnp.bfloat16)
-    return result, gathered
-
-
-def on_device(
-    query_in,
-    key_in,
-    value_in,
-    erase_pre,
-    decay_pre,
-    mix_gain,
-    expert_in,
-    expert_gain,
-    routes,
-    route_weight,
-    gate_weight,
-    up_weight,
-    down_weight,
-):
-    reads, local, steps, maps = mixer_local(query_in, key_in, value_in, erase_pre, decay_pre)
-
-    def hold(arrived):
-        held, sent = lax.optimization_barrier((arrived, maps.astype(jnp.bfloat16)))
-        return held, lax.all_gather(sent, "ep")
-
-    expert_out, gathered = expert_half(
-        hold, expert_in, expert_gain, routes, route_weight, gate_weight, up_weight, down_weight
-    )
-    mixer_out = mixer_finish(gathered, steps, reads, local, mix_gain)
-    return (mixer_out, expert_out)
+    result = jnp.dot(combine, returned.astype(jnp.float32), precision=highest)
+    return (mixer_out, result.astype(jnp.bfloat16))
 
 
 def solution(mesh):

time: 189 us -> 133 us (0.70)
  waiting for transfers between devices: 57.8 us -> 0 us
  Pallas kernels: 53.5 us -> 99.4 us
  blocking collectives: 27.2 us -> 0 us
  between operations: 13.9 us -> 0.74 us
  starting transfers between devices: 4.89 us -> 0 us
    reduce_scatter x1 -> x0, waiting for transfers between devices: 46.5 us -> none  [expert_half(): lax.psum_scatter(partial_sum, 'tp', scatter_dimension=0, tiled=True)]
    pallas_call x2, Pallas kernels: 53.5 us -> 99.4 us  [the longest x1 54.6 us: outbound(): pl.pallas_call(functools.partial(outbound_kernel, ep_count, tp_count), in...]
    all_to_all x1 -> x0, blocking collectives: 27.2 us -> none  [expert_half(): lax.all_to_all(buffer.reshape(experts_n, capacity, col_count), 'ep', spli...]
    all_to_all x1 -> x0, waiting for transfers between devices: 8.89 us -> none  [expert_half(): lax.all_to_all(summed.reshape(col_count, experts_n, capacity), 'ep', spli...]
    all_to_all x1 -> x0, starting transfers between devices: 4.59 us -> none  [expert_half(): lax.all_to_all(summed.reshape(col_count, experts_n, capacity), 'ep', spli...]
    all_gather x2 -> x0, waiting for transfers between devices: 2.35 us -> none  [the longest x1 2.35 us: hold(): return (held, lax.all_gather(sent, 'ep'))]
  transfers between devices with their start and end apart: 4 -> 0, of which waited for: 3 -> 0; matrix products, arithmetic and copies ran while one was open for 12% -> 0% of each run, Pallas kernels for 28% -> 0%
where the time goes in v1:
time: 133 us
  Pallas kernels  99.4 us (75%)
  matrix products  24.1 us (18%)
  other arithmetic  4.27 us (3%)
  local copies, waits for them, and re-layouts  3.99 us (3%)
    pallas_call x1, Pallas kernels, outbound(): pl.pallas_call(functools.partial(outbound_kernel, ep_count, tp_count), in...  54.6 us
    pallas_call x1, Pallas kernels, inbound(): pl.pallas_call(functools.partial(inbound_kernel, ep_count, tp_count), in_...  44.8 us
    dot_general x1, matrix products, on_device(): jnp.dot(hidden, down_weight[0], preferred_element_type=jnp.float32)  12.1 us
    dot_general x1, matrix products, on_device(): up_sum = jnp.dot(arrived, up_weight[0], preferred_element_type=jnp.float32)  8 us

profile of v1, /device:TPU:0, one launch (start us, length us, event | category | flops | bytes accessed | tf_op | source)
XLA Modules:
  0.0 132.5 jit_solution(10512942828349309351)
XLA Ops:
  0.6 0.0 copy-start
  0.6 0.8 dynamic-slice
  1.5 0.8 copy.31
  2.3 0.1 eq.56
  2.5 1.1 reduce-window.6
  3.6 0.2 slice_reduce_fusion
  3.9 0.1 eq.52
  4.0 0.1 fusion.20
  4.1 0.1 reshape.53
  4.3 0.1 copy.33
  4.3 0.7 multiply_add_fusion
  5.0 0.3 convert_reduce_fusion
  5.4 1.5 %convert_element_type.38 = f32[256,2048]{1,0:T(8,128)S(1)} convert(bf16[256,2048]{1,0:T(8,128)(2,1)} %param.19) | non-fusion elementwise | flops 524288 | bytes 3145728 | tf_op jit(solution)/shard_map/convert_element_type | solution.py:506
  6.8 0.0 copy-done
  6.8 0.3 multiply_reduce_fusion
  7.1 1.3 %convolution_convert_fusion = bf16[768,512]{1,0:T(8,128)(2,1)} fusion(bf16[768,256]{1,0:T(8,128)(2,1)S(1)} %convert_reduce_fusion, f32[256,2048]{1,0:T(8,128)S(1)} %convert_element_type.38, s32[]{:T(128)S(6)} %select_n.3, f32[512]{0:T(512)S(1)} %dynamic-slice, f32[256]{0:T(256)S(1)} %add_rsqrt_fusion), kind=kOutput, calls=%fused_computation.13 | convolution fusion | flops 202113024 | bytes 1707012 | tf_op jit(solution)/shard_map/dot_general | solution.py:515
  8.5 54.6 %outbound.1 = (bf16[8,96,2048]{2,1,0:T(8,128)(2,1)}, bf16[2,256,1024]{2,1,0:T(8,128)(2,1)}, f32[256,1024]{1,0:T(8,128)}, f32[8,2,4,64,128]{4,3,2,1,0:T(8,128)}, bf16[2,4,64,128]{3,2,1,0:T(8,128)(2,1)}) custom-call(bf16[8,96,512]{2,1,0:T(8,128)(2,1)} %bitcast.34, bf16[256,1024]{1,0:T(8,128)(2,1)} %q_ref.1, bf16[256,1024]{1,0:T(8,128)(2,1)} %k_ref.1, ...), custom_call_target="tpu_custom_call" | custom-call | flops 40000000000 | bytes 8388608 | tf_op jit(solution)/shard_map/outbound/pallas_call | solution.py:406
  63.1 8.0 %fusion.2 = f32[768,896]{1,0:T(8,128)} fusion(bf16[768,2048]{1,0:T(8,128)(2,1)} %bitcast.37, bf16[1,2048,896]{2,1,0:T(8,128)(2,1)} %param.24), kind=kOutput, calls=%fused_computation.2 | convolution fusion | flops 2818572288 | bytes 9568256 | tf_op jit(solution)/shard_map/dot_general | solution.py:524
  71.1 0.0 copy-start.3
  71.1 12.1 %fusion.6 = bf16[768,2048]{1,0:T(8,128)(2,1)} fusion(bf16[1,896,2048]{2,1,0:T(8,128)(2,1)} %param.25, f32[768,896]{1,0:T(8,128)} %fusion.2, bf16[768,2048]{1,0:T(8,128)(2,1)} %bitcast.38, bf16[1,2048,896]{2,1,0:T(8,128)(2,1)} %param.23), kind=kOutput, calls=%fused_computation.6 | convolution fusion | flops 5642846208 | bytes 16384000 | tf_op jit(solution)/shard_map/dot_general | solution.py:526
  83.2 0.0 copy-done.3
  83.2 0.8 copy.34.gain_ref
  84.0 0.0 copy-start.2
  84.0 44.8 %inbound.1 = (bf16[256,1024]{1,0:T(8,128)(2,1)}, bf16[8,96,512]{2,1,0:T(8,128)(2,1)}) custom-call(bf16[8,96,2048]{2,1,0:T(8,128)(2,1)} %bitcast.36, bf16[2,4,64,128]{3,2,1,0:T(8,128)(2,1)} %get-tuple-element.10.maps_ref, f32[8,2,4,64,128]{4,3,2,1,0:T(8,128)} %get-tuple-element.11.step_ref, bf16[2,256,1024]{2,1,0:T(8,128)(2,1)} %get-tuple-element.12.read_ref, ...), custom_call_target="tpu_custom_call" | custom-call | flops 10000000000 | bytes 8388608 | tf_op jit(solution)/shard_map/inbound/pallas_call | solution.py:443
  128.8 0.0 copy-start.1
  128.8 0.0 copy-done.2
  128.9 0.2 select_reduce_fusion
  129.1 2.6 %convolution_convert_fusion.1 = bf16[256,512]{1,0:T(8,128)(2,1)} fusion(f32[256,768]{1,0:T(8,128)S(1)} %select_reduce_fusion, bf16[768,512]{1,0:T(8,128)(2,1)} %bitcast.33), kind=kOutput, calls=%fused_computation.14 | convolution fusion | flops 1208090624 | bytes 1835008 | tf_op jit(solution)/shard_map/dot_general | solution.py:533
  131.7 0.0 copy-done.1
  131.7 0.8 copy.36
  (4 shorter events, 0.1 us)
Async XLA Ops:
  0.6 6.2 %copy-start = (bf16[256,2048]{1,0:T(8,128)(2,1)S(1)}, bf16[256,2048]{1,0:T(8,128)(2,1)}, u32[]{:S(2)}) copy-start(bf16[256,2048]{1,0:T(8,128)(2,1)} %param.19) | copy-start | bytes 3145732
  71.1 12.1 %copy-start.3 = (f32[256]{0:T(256)S(1)}, f32[256]{0:T(256)}, u32[]{:S(2)}) copy-start(f32[256]{0:T(256)} %param.18) | copy-start | bytes 3076
  84.0 44.8 %copy-start.2 = (f32[256,2]{0,1:T(2,128)S(1)}, f32[256,2]{0,1:T(2,128)}, u32[]{:S(2)}) copy-start(f32[256,2]{0,1:T(2,128)} %param.22) | copy-start | bytes 6148
  128.8 2.9 %copy-start.1 = (bf16[256,1024]{1,0:T(8,128)(2,1)S(1)}, bf16[256,1024]{1,0:T(8,128)(2,1)}, u32[]{:S(2)}) copy-start(bf16[256,1024]{1,0:T(8,128)(2,1)} %get-tuple-element.18) | copy-start | bytes 1572868
